TPU v7x, 32 devices: a whole 2x2x4 slice. The times are simulated.
32 devices in a mesh: rep: 4 (over z), fs: 4 (over y, x), tp: 2 (over core).
Axes of the slice: x: 2, y: 2, z: 4, core: 2. Of those that a mesh axis runs over, the one named last changes fastest.
Arguments:
- hidden_pre: bfloat16 [8192, 4096], P(('rep', 'fs'), 'tp'), may hold values from -6 to 6
- out_grad: bfloat16 [8192, 2048], P(('rep', 'fs')), may hold values from -8 to 8
- down_weight: bfloat16 [2048, 4096], P('fs', 'tp'), may hold values from -0.09375 to 0.09375
Outputs:
- hidden_grad: bfloat16 [8192, 4096], P(('rep', 'fs'), 'tp')
- weight_grad: float32 [2048, 4096], P('fs', 'tp')
All inputs are finite; a program needn't handle non-finite values.
Results may differ from a plain program's by a relative error of at most 0.0049.
Values may be sent and summed in bfloat16 or wider, within the bound.
A program may use at most 64 MiB of HBM per device.

v0:
```python
import math
import jax
import jax.numpy as jnp
from jax import lax
from jax.sharding import PartitionSpec as P


def body(hidden_pre, out_grad, down_weight):
    rows = hidden_pre.shape[0]
    ff_local = hidden_pre.shape[1]
    back = jnp.dot(
        out_grad,
        lax.all_gather(down_weight, "fs", axis=0, tiled=True),
        preferred_element_type=jnp.float32,
    )
    positive = jnp.maximum(hidden_pre.astype(jnp.float32), 0.0)
    hidden_grad = (2.0 * positive * back).astype(jnp.bfloat16)
    act = (positive * positive).astype(jnp.bfloat16)
    partial_value = lax.dot_general(
        out_grad, act, (((0,), (0,)), ((), ())), preferred_element_type=jnp.float32
    )
    partial_value = partial_value.astype(jnp.bfloat16)
    received = lax.all_to_all(partial_value, "fs", split_axis=0, concat_axis=0, tiled=True)
    groups = lax.axis_size("fs")
    local_sum = jnp.sum(
        received.reshape(groups, received.shape[0] // groups, ff_local), axis=0, dtype=jnp.float32
    )
    total = lax.psum(local_sum, "rep")
    tokens_all = rows * lax.axis_size("rep") * groups
    weight_grad = total * (1.0 / math.sqrt(tokens_all))
    return (hidden_grad, weight_grad)


def solution(mesh):
    placed = (P(("rep", "fs"), "tp"), P(("rep", "fs"), None), P("fs", "tp"))
    return jax.shard_map(
        body,
        mesh=mesh,
        in_specs=placed,
        out_specs=(P(("rep", "fs"), "tp"), P("fs", "tp")),
        check_vma=False,
    )
```

profile of v0, /device:TPU:0, one launch (start us, length us, event | category | flops | bytes accessed | tf_op | source)
XLA Modules:
  0.0 297.2 jit_solution(1170586137731124309)
XLA Ops:
  8.0 0.0 copy-start
  8.0 0.0 all-reduce.2.cloned.1.call-start
  8.1 1.5 copy-done
  9.6 8.3 %convolution_convert_fusion = bf16[2048,2048]{0,1:T(8,128)(2,1)} fusion(bf16[512,2048]{1,0:T(8,128)(2,1)S(1)} %copy-done, bf16[512,2048]{1,0:T(8,128)(2,1)} %param.3), kind=kOutput, calls=%fused_computation.1 | convolution fusion | flops 4303355904 | bytes 12582912 | tf_op jit(solution)/shard_map/dot_general | solution.py:19
  17.9 98.5 %all_to_all.9 = bf16[4,512,2048]{2,1,0:T(8,128)(2,1)S(1)} all-to-all(bf16[4,512,2048]{2,1,0:T(8,128)(2,1)} %bitcast.6), channel_id=1, replica_groups=mesh['rep'=4,'fs'=4,'tp'=2] {'fs'}, dimensions={0} | all-to-all | bytes 16777216 | tf_op jit(solution)/shard_map/all_to_all | solution.py:23
  116.4 3.9 %convert_reduce_fusion = f32[512,2048]{1,0:T(8,128)} fusion(bf16[4,512,2048]{2,1,0:T(8,128)(2,1)S(1)} %all_to_all.9), kind=kLoop, calls=%fused_computation | loop fusion | flops 7340032 | bytes 12582912 | tf_op jit(solution)/shard_map/reduce_sum | solution.py:25
  120.3 0.0 all-reduce.2.cloned.1.call-update
  120.3 0.0 all-gather.2.cloned.1.call-start
  120.4 0.5 all-gather.2.cloned.1.call-update
  120.9 154.4 %all-reduce.2.cloned.1.call-done = f32[512,2048]{1,0:T(8,128)} async-done(((f32[512,2048]{1,0:T(8,128)}), f32[512,2048]{1,0:T(8,128)}) %all-reduce.2.cloned.1.call-update) | async-done | bytes 4194320 | tf_op jit(solution)/shard_map/psum | solution.py:28
  275.4 5.0 %broadcast_multiply_fusion = f32[512,2048]{1,0:T(8,128)} fusion(f32[512,2048]{1,0:T(8,128)} %all-reduce.2.cloned.1.call-done), kind=kLoop, calls=%fused_computation.5 | loop fusion | flops 1048576 | bytes 8388608 | tf_op jit(solution)/shard_map/mul | solution.py:30
  280.3 0.0 all-gather.2.cloned.1.call-done
  280.3 9.5 %multiply_convert_fusion.1 = bf16[512,2048]{1,0:T(8,128)(2,1)} fusion(bf16[512,2048]{1,0:T(8,128)(2,1)} %param.3, bf16[512,2048]{1,0:T(8,128)(2,1)S(1)} %copy-done, bf16[2048,2048]{1,0:T(8,128)(2,1)} %all-gather.2.cloned.1.call-done), kind=kOutput, calls=%fused_computation.3 | convolution fusion | flops 4300210176 | bytes 14680064 | tf_op jit(solution)/shard_map/dot_general | solution.py:11
Async XLA Ops:
  8.0 1.6 copy-start
  8.0 267.3 %all-reduce.2.cloned.1.call-start = ((), (), s32[]{:S(2)}) async-start(), calls=%async_computation.2 | async-start | bytes 8388608 | tf_op jit(solution)/shard_map/psum | solution.py:28
  120.3 160.0 %all-gather.2.cloned.1.call-start = ((), (), s32[]{:S(2)}) async-start(), calls=%async_computation.1 | async-start | bytes 10485760 | tf_op jit(solution)/shard_map/all_gather | solution.py:13
Sparse Core Ops, SparseCore 0:
  120.4 154.8 all-reduce.1
Sparse Core Ops, SparseCore 1:
  122.7 87.2 all-gather.1
where the time goes:
time: 297 us
  waiting for transfers between devices  155 us (52%)
  blocking collectives  98.5 us (33%)
  matrix products  17.8 us (6%)
  between operations  15.5 us (5%)
  other arithmetic  8.83 us (3%)
    psum x1, waiting for transfers between devices, body(): total = lax.psum(local_sum, 'rep')  154 us
    all_to_all x1, blocking collectives, body(): lax.all_to_all(partial_value, 'fs', split_axis=0, concat_axis=0, tiled=True)  98.5 us
    dot_general x1, matrix products, body(): jnp.dot(out_grad, lax.all_gather(down_weight, 'fs', axis=0, tiled=True),...  9.45 us
    dot_general x1, matrix products, body(): lax.dot_general(out_grad, act, (((0,), (0,)), ((), ())), preferred_elemen...  8.35 us
  transfers between devices with their start and end apart: 2, of which 1 were waited for; matrix products, arithmetic and copies ran while one was open for 2% of the time, Pallas kernels for 0%

commit v1 on v0

--- a/solution.py
+++ b/solution.py
@@ -25,7 +25,7 @@
     local_sum = jnp.sum(
         received.reshape(groups, received.shape[0] // groups, ff_local), axis=0, dtype=jnp.float32
     )
-    total = lax.psum(local_sum, "rep")
+    total = jnp.sum(lax.all_gather(local_sum, "rep"), axis=0)
     tokens_all = rows * lax.axis_size("rep") * groups
     weight_grad = total * (1.0 / math.sqrt(tokens_all))
     return (hidden_grad, weight_grad)

time: 297 us -> 494 us (1.66)
  waiting for transfers between devices: 155 us -> 283 us
  blocking collectives: 98.5 us -> 159 us
  other arithmetic: 8.83 us -> 19 us
    all_gather x0 -> x1, waiting for transfers between devices: none -> 279 us  [body(): total = jnp.sum(lax.all_gather(local_sum, 'rep'), axis=0)]
    psum x1 -> x0, waiting for transfers between devices: 154 us -> none  [body(): total = lax.psum(local_sum, 'rep')]
    all_to_all x1, blocking collectives: 98.5 us -> 159 us  [body(): lax.all_to_all(partial_value, 'fs', split_axis=0, concat_axis=0, tiled=True)]
    reduce_sum x0 -> x1, other arithmetic: none -> 10.2 us  [body(): total = jnp.sum(lax.all_gather(local_sum, 'rep'), axis=0)]
  transfers between devices with their start and end apart: 2 -> 2, of which waited for: 1 -> 2; matrix products, arithmetic and copies ran while one was open for 2% -> 4% of each run, Pallas kernels for 0% -> 0%
where the time goes in v1:
time: 494 us; the launch traced here: 493 us
  waiting for transfers between devices  283 us (57%)
  blocking collectives  159 us (32%)
  other arithmetic  19 us (4%)
  matrix products  17.8 us (4%)
  between operations  14 us (3%)
    all_gather x1, waiting for transfers between devices, body(): total = jnp.sum(lax.all_gather(local_sum, 'rep'), axis=0)  279 us
    all_to_all x1, blocking collectives, body(): lax.all_to_all(partial_value, 'fs', split_axis=0, concat_axis=0, tiled=True)  159 us
    reduce_sum x1, other arithmetic, body(): total = jnp.sum(lax.all_gather(local_sum, 'rep'), axis=0)  10.2 us
  transfers between devices with their start and end apart: 2, of which 2 were waited for; matrix products, arithmetic and copies ran while one was open for 4% of the time, Pallas kernels for 0%

profile of v1, /device:TPU:0, one launch (start us, length us, event | category | flops | bytes accessed | tf_op | source)
XLA Modules:
  0.0 493.3 jit_solution(6879388479122855075)
XLA Ops:
  7.2 0.0 copy-start
  7.2 0.0 all-gather.4.cloned.1.call-start
  7.2 0.7 all-gather.4.cloned.1.call-update
  7.9 0.0 all-gather.6.cloned.1.call-start
  8.0 0.8 copy-done
  8.8 8.3 %convolution_convert_fusion = bf16[2048,2048]{0,1:T(8,128)(2,1)} fusion(bf16[512,2048]{1,0:T(8,128)(2,1)S(1)} %copy-done, bf16[512,2048]{1,0:T(8,128)(2,1)} %param.3), kind=kOutput, calls=%fused_computation.1 | convolution fusion | flops 4303355904 | bytes 12582912 | tf_op jit(solution)/shard_map/dot_general | solution.py:19
  17.1 158.8 %all_to_all.9 = bf16[4,512,2048]{2,1,0:T(8,128)(2,1)S(1)} all-to-all(bf16[4,512,2048]{2,1,0:T(8,128)(2,1)} %bitcast.8), channel_id=1, replica_groups=mesh['rep'=4,'fs'=4,'tp'=2] {'fs'}, dimensions={0} | all-to-all | bytes 16777216 | tf_op jit(solution)/shard_map/all_to_all | solution.py:23
  175.9 3.9 convert_reduce_fusion
  179.7 0.0 all-gather.6.cloned.1.call-update
  179.8 2.6 all-gather.4.cloned.1.call-done
  182.4 9.5 %multiply_convert_fusion.1 = bf16[512,2048]{1,0:T(8,128)(2,1)} fusion(bf16[512,2048]{1,0:T(8,128)(2,1)} %param.3, bf16[512,2048]{1,0:T(8,128)(2,1)S(1)} %copy-done, bf16[2048,2048]{1,0:T(8,128)(2,1)} %all-gather.4.cloned.1.call-done), kind=kOutput, calls=%fused_computation.3 | convolution fusion | flops 4300210176 | bytes 14680064 | tf_op jit(solution)/shard_map/dot_general | solution.py:11
  191.8 279.5 %all-gather.6.cloned.1.call-done = f32[2048,2048]{1,0:T(8,128)} async-done(((f32[512,2048]{1,0:T(8,128)}), f32[2048,2048]{1,0:T(8,128)}) %all-gather.6.cloned.1.call-update) | async-done | bytes 16777232 | tf_op jit(solution)/shard_map/all_gather | solution.py:28
  471.3 10.2 %reduce_sum.19 = f32[512,2048]{1,0:T(8,128)} reduce(f32[4,512,2048]{2,1,0:T(8,128)} %bitcast.7, f32[]{:T(128)} %constant.3.clone.1), dimensions={0}, to_apply=%region_1.0 | reduce | flops 3145728 | bytes 20971524 | tf_op jit(solution)/shard_map/reduce_sum | solution.py:28
  481.5 5.0 %broadcast_multiply_fusion = f32[512,2048]{1,0:T(8,128)} fusion(f32[512,2048]{1,0:T(8,128)} %reduce_sum.19), kind=kLoop, calls=%fused_computation.5 | loop fusion | flops 1048576 | bytes 8388608 | tf_op jit(solution)/shard_map/mul | solution.py:30
Async XLA Ops:
  7.2 1.6 copy-start
  7.2 175.2 %all-gather.4.cloned.1.call-start = ((), (), s32[]{:S(2)}) async-start(), calls=%async_computation.1 | async-start | bytes 10485760 | tf_op jit(solution)/shard_map/all_gather | solution.py:13
  7.9 463.4 %all-gather.6.cloned.1.call-start = ((), (), s32[]{:S(2)}) async-start(), calls=%async_computation.2 | async-start | bytes 20971520 | tf_op jit(solution)/shard_map/all_gather | solution.py:28
Sparse Core Ops, SparseCore 0:
  9.8 172.5 all-gather.3
  184.5 286.7 all-gather.5
